TPU v7x, 32 devices: a whole 2x2x4 slice. The times are simulated.
32 devices in a mesh: sp: 16 (over z, y, x), tp: 2 (over core).
Axes of the slice: x: 2, y: 2, z: 4, core: 2. Of those that a mesh axis runs over, the one named last changes fastest.
Arguments:
- resid: bfloat16 [6144, 2048], P('sp', 'tp'), may hold values from -40 to 40
- query_one: bfloat16 [6144, 1024], P('sp', 'tp'), may hold values from -64 to 64
- key_one: bfloat16 [6144, 1024], P('sp', 'tp'), may hold values from -64 to 64
- query_two: bfloat16 [6144, 1024], P('sp', 'tp'), may hold values from -64 to 64
- key_two: bfloat16 [6144, 1024], P('sp', 'tp'), may hold values from -64 to 64
- values: bfloat16 [6144, 2048], P('sp', 'tp'), may hold values from -6 to 6
- mix_lambda: float32 [8], P('tp'), may hold values from 0.3 to 0.8
- segments: int32 [6144], P('sp'), may hold values from 0 to 7, never falling along the last dimension, each value on 1 to 1536 neighbouring positions
- head_gain: float32 [256], replicated, may hold values from 0.1 to 1.9
- out_weight: bfloat16 [2048, 2048], P(None, 'tp'), may hold values from -0.125 to 0.125
- mixer_gain: float32 [2048], P('tp'), may hold values from 0.1 to 1.9
- gate_weight: bfloat16 [2048, 6144], P('sp', 'tp'), may hold values from -0.125 to 0.125
- up_weight: bfloat16 [2048, 6144], P('sp', 'tp'), may hold values from -0.125 to 0.125
- down_weight: bfloat16 [6144, 2048], P('tp', 'sp'), may hold values from -0.078125 to 0.078125
Outputs:
- layer_out: bfloat16 [6144, 2048], P('sp', 'tp')
Inputs may be any that keep to these rules, and one draw needn't show every extreme that they name: `segments`: numbers never fall along the sequence; each document has at most 1536 positions and one has exactly that many.
All inputs are finite; a program needn't handle non-finite values.
Results may differ from a plain program's by a relative error of at most 0.012.
Values may be sent and summed in bfloat16 or wider, within the bound.
A program may use at most 128 MiB of HBM per device.

v0:
```python
import jax
import jax.numpy as jnp
from jax import lax
from jax.sharding import PartitionSpec as P

HD = 128
VD = 256
REACH = 4


def shifted(value, axis, by):
    length = lax.axis_size(axis)
    pairs = [(i, i + by) for i in range(length) if 0 <= i + by < length]
    return lax.ppermute(value, axis, pairs)


def body(
    resid,
    query_one,
    key_one,
    query_two,
    key_two,
    values,
    mix_lambda,
    segments,
    head_gain,
    out_weight,
    mixer_gain,
    gate_weight,
    up_weight,
    down_weight,
):
    rows = query_one.shape[0]
    heads = mix_lambda.shape[0]
    position = lax.axis_index("sp")
    carried = (key_one, key_two, values, segments)
    earlier = [carried]
    for step in range(REACH):
        carried = shifted((carried[0], carried[1], carried[2], carried[3]), "sp", 1)
        earlier.insert(0, carried)
    width = (REACH + 1) * rows
    k_first = jnp.concatenate([piece[0] for piece in earlier], 0).reshape(width, heads, HD)
    k_second = jnp.concatenate([piece[1] for piece in earlier], 0).reshape(width, heads, HD)
    vals = jnp.concatenate([piece[2] for piece in earlier], 0).reshape(width, heads, VD)
    seg_key = jnp.concatenate([piece[3] for piece in earlier], 0)
    q_pos = position * rows + jnp.arange(rows, dtype=jnp.int32)
    k_pos = (position - REACH) * rows + jnp.arange(width, dtype=jnp.int32)
    allowed = (
        (seg_key[None, :] == segments[:, None])
        & (k_pos[None, :] <= q_pos[:, None])
        & (k_pos[None, :] >= 0)
    )

    def weights(query, keys):
        score = jnp.einsum(
            "qhd,khd->hqk", query.reshape(rows, heads, HD), keys, preferred_element_type=jnp.float32
        ) * HD ** (-0.5)
        score = jnp.where(allowed[None], score, -jnp.inf)
        score = score - jnp.max(score, axis=-1, keepdims=True)
        expo = jnp.exp(score)
        return (expo / jnp.sum(expo, axis=-1, keepdims=True)).astype(jnp.bfloat16)

    out_first = jnp.einsum(
        "hqk,khe->qhe", weights(query_one, k_first), vals, preferred_element_type=jnp.float32
    )
    out_second = jnp.einsum(
        "hqk,khe->qhe", weights(query_two, k_second), vals, preferred_element_type=jnp.float32
    )
    head_out = out_first - mix_lambda[None, :, None] * out_second
    meansq = jnp.mean(head_out * head_out, axis=-1, keepdims=True)
    attn_rows = (
        (head_out * lax.rsqrt(meansq + 1e-05) * head_gain)
        .reshape(rows, heads * VD)
        .astype(jnp.bfloat16)
    )
    projected = jnp.dot(
        lax.all_gather(attn_rows, "tp", axis=1, tiled=True),
        out_weight,
        preferred_element_type=jnp.float32,
    )
    mid = (resid.astype(jnp.float32) + projected).astype(jnp.bfloat16)
    midf = mid.astype(jnp.float32)
    squares = lax.psum(jnp.sum(midf * midf, axis=1), "tp")
    channels = mid.shape[1] * lax.axis_size("tp")
    normed = (midf * lax.rsqrt(squares / channels + 1e-06)[:, None] * mixer_gain).astype(
        jnp.bfloat16
    )
    whole_rows = lax.all_gather(normed, "tp", axis=1, tiled=True)
    gate = jnp.dot(
        whole_rows,
        lax.all_gather(gate_weight, "sp", axis=0, tiled=True),
        preferred_element_type=jnp.float32,
    )
    up = jnp.dot(
        whole_rows,
        lax.all_gather(up_weight, "sp", axis=0, tiled=True),
        preferred_element_type=jnp.float32,
    )
    hidden = (jax.nn.silu(gate) * up).astype(jnp.bfloat16)
    terms = jnp.dot(
        hidden,
        lax.all_gather(down_weight, "sp", axis=1, tiled=True),
        preferred_element_type=jnp.float32,
    )
    summed = lax.psum_scatter(
        terms.astype(jnp.bfloat16), "tp", scatter_dimension=1, tiled=True
    ).astype(jnp.float32)
    return (midf + summed).astype(jnp.bfloat16)


def solution(mesh):
    in_specs = (
        P("sp", "tp"),
        P("sp", "tp"),
        P("sp", "tp"),
        P("sp", "tp"),
        P("sp", "tp"),
        P("sp", "tp"),
        P("tp"),
        P("sp"),
        P(),
        P(None, "tp"),
        P("tp"),
        P("sp", "tp"),
        P("sp", "tp"),
        P("tp", "sp"),
    )
    out_specs = P("sp", "tp")
    return jax.shard_map(body, mesh=mesh, in_specs=in_specs, out_specs=out_specs, check_vma=False)
```

profile of v0, /device:TPU:0, one launch (start us, length us, event | category | flops | bytes accessed | tf_op | source)
XLA Modules:
  0.0 768.8 jit_solution(17959958012359783923)
XLA Ops:
  7.8 4.9 collective-permute-start.12
  31.0 16.5 %collective-permute-done.5 = s32[384]{0:T(512)S(1)} collective-permute-done((s32[384]{0:T(512)S(1)}, s32[384]{0:T(512)S(1)}, u32[]{:S(2)}, u32[]{:S(2)}) %collective-permute-start.5) | collective-permute-done | bytes 1568 | tf_op jit(solution)/shard_map/ppermute | solution.py:14
  64.9 5.1 collective-permute-start.14
  74.4 5.9 collective-permute-start.10
  82.8 5.1 collective-permute-start.15
  90.5 5.3 collective-permute-start.1
  102.2 6.2 fusion.19
  108.4 17.4 %fusion.30 = (f32[4,384]{1,0:T(4,128)S(1)}, f32[4,384,1920]{1,2,0:T(8,128)}) fusion(f32[4,1920,384]{2,1,0:T(8,128)} %fusion.19, pred[384,1920]{0,1:T(8,128)(4,1)S(1)} %and_and_fusion), kind=kOutput, calls=%fused_computation.71 | output fusion | flops 17696640 | bytes 24336384 | tf_op jit(solution)/shard_map/sub | solution.py:59
  125.7 5.6 collective-permute-start.2
  134.7 6.1 fusion.22
  143.1 5.5 collective-permute-start.3
  148.6 17.7 %fusion.31 = (f32[4,384]{1,0:T(4,128)S(1)}, f32[4,384,1920]{1,2,0:T(8,128)}) fusion(f32[4,1920,384]{2,1,0:T(8,128)} %fusion.22, pred[384,1920]{0,1:T(8,128)(4,1)} %copy-done.4), kind=kOutput, calls=%fused_computation.72 | output fusion | flops 17696640 | bytes 24336384 | tf_op jit(solution)/shard_map/sub | solution.py:59
  171.1 6.3 copy.20
  177.4 8.0 %fusion.9 = f32[4,256,384]{2,1,0:T(8,128)S(1)} fusion(bf16[1920,4,256]{0,2,1:T(8,128)(2,1)} %bitcast.60, f32[4,384,1920]{1,2,0:T(8,128)} %get-tuple-element.6, f32[4,384]{1,0:T(4,128)S(1)} %get-tuple-element.5), kind=kOutput, calls=%fused_computation.15 | convolution fusion | flops 1515847680 | bytes 17307648 | tf_op jit(solution)/shard_map/hqk,khe->qhe/dot_general | solution.py:66
  185.4 6.8 fusion.16
  193.6 14.5 %all-gather.6.cloned.1.call-done = bf16[384,2048]{0,1:T(8,128)(2,1)} async-done(((bf16[384,1024]{0,1:T(8,128)(2,1)}), bf16[384,2048]{0,1:T(8,128)(2,1)}) %all-gather.6.cloned.1.call-update) | async-done | bytes 1572880 | tf_op jit(solution)/shard_map/all_gather | solution.py:77
  208.1 4.6 fusion.12
  218.3 9.2 %all-gather.8.cloned.1.call-done = bf16[384,2048]{1,0:T(8,128)(2,1)} async-done(((bf16[384,1024]{1,0:T(8,128)(2,1)}), bf16[384,2048]{1,0:T(8,128)(2,1)}) %all-gather.8.cloned.1.call-update) | async-done | bytes 1572880 | tf_op jit(solution)/shard_map/all_gather | solution.py:88
  227.5 155.4 %all-gather.10.cloned.1.call-done = bf16[2048,3072]{1,0:T(8,128)(2,1)} async-done(((bf16[128,3072]{1,0:T(8,128)(2,1)}), bf16[2048,3072]{1,0:T(8,128)(2,1)}) %all-gather.10.cloned.1.call-update) | async-done | bytes 12582928 | tf_op jit(solution)/shard_map/all_gather | solution.py:91
  382.9 9.9 %fusion.32 = f32[384,3072]{1,0:T(8,128)} fusion(bf16[384,2048]{1,0:T(8,128)(2,1)} %all-gather.8.cloned.1.call-done, bf16[2048,3072]{1,0:T(8,128)(2,1)} %all-gather.10.cloned.1.call-done), kind=kOutput, calls=%fused_computation.73 | convolution fusion | flops 4831838208 | bytes 18874368 | tf_op jit(solution)/shard_map/dot_general | solution.py:89
  392.7 142.4 %all-gather.12.cloned.1.call-done = bf16[2048,3072]{1,0:T(8,128)(2,1)} async-done(((bf16[128,3072]{1,0:T(8,128)(2,1)}), bf16[2048,3072]{1,0:T(8,128)(2,1)}) %all-gather.12.cloned.1.call-update) | async-done | bytes 12582928 | tf_op jit(solution)/shard_map/all_gather | solution.py:96
  535.1 196.2 %all-gather.14.cloned.1.call-done = bf16[3072,2048]{1,0:T(8,128)(2,1)} async-done(((bf16[3072,128]{1,0:T(8,128)(2,1)}), bf16[3072,2048]{1,0:T(8,128)(2,1)}) %all-gather.14.cloned.1.call-update) | async-done | bytes 12582928 | tf_op jit(solution)/shard_map/all_gather | solution.py:102
  731.3 21.0 %convolution_convert_fusion = bf16[384,2048]{1,0:T(8,128)(2,1)} fusion(bf16[3072,2048]{1,0:T(8,128)(2,1)} %all-gather.14.cloned.1.call-done, f32[384,3072]{1,0:T(8,128)} %fusion.32, bf16[384,2048]{1,0:T(8,128)(2,1)S(1)} %copy-done.13, bf16[2048,3072]{1,0:T(8,128)(2,1)} %all-gather.12.cloned.1.call-done), kind=kOutput, calls=%fused_computation.20 | convolution fusion | flops 9671540736 | bytes 33030144 | tf_op jit(solution)/shard_map/dot_general | solution.py:100
  752.3 7.3 reduce-scatter.2.cloned.1.call-done
  (101 shorter events, 72.3 us)
Async XLA Ops:
  6.5 95.7 %copy-start = (bf16[384,512]{1,0:T(8,128)(2,1)S(1)}, bf16[384,512]{1,0:T(8,128)(2,1)}, u32[]{:S(2)}) copy-start(bf16[384,512]{1,0:T(8,128)(2,1)} %param.17) | copy-start | bytes 1179652
  6.5 201.5 %all-gather.6.cloned.1.call-start = ((), (), s32[]{:S(2)}) async-start(), calls=%async_computation.1 | async-start | bytes 2359296 | tf_op jit(solution)/shard_map/all_gather | solution.py:77
  7.8 19.7 %collective-permute-start.12 = (bf16[384,512]{0,1:T(8,128)(2,1)S(1)}, bf16[384,512]{0,1:T(8,128)(2,1)S(1)}, u32[]{:S(2)}, u32[]{:S(2)}) collective-permute-start(bf16[384,512]{0,1:T(8,128)(2,1)S(1)} %copy.26), channel_id=1, source_target_pairs={{0,2},{2,4},{4,6},{6,8},{8,10},{10,12},{12,14},{14,16},{16,18},{18... | collective-permute-start | bytes 1179656 | tf_op jit(solution)/shard_map/ppermute | solution.py:14
  12.7 11.4 %collective-permute-start.4 = (s32[384]{0:T(512)}, s32[384]{0:T(512)S(1)}, u32[]{:S(2)}, u32[]{:S(2)}) collective-permute-start(s32[384]{0:T(512)} %param.21), channel_id=1, source_target_pairs={{0,2},{2,4},{4,6},{6,8},{8,10},{10,12},{12,14},{14,16},{16,18},{18... | collective-permute-start | bytes 4616 | tf_op jit(solution)/shard_map/ppermute | solution.py:14
  16.1 74.4 %collective-permute-start = (bf16[384,1024]{1,0:T(8,128)(2,1)}, bf16[384,1024]{1,0:T(8,128)(2,1)S(1)}, u32[]{:S(2)}, u32[]{:S(2)}) collective-permute-start(bf16[384,1024]{1,0:T(8,128)(2,1)} %param.19), channel_id=1, source_target_pairs={{0,2},{2,4},{4,6},{6,8},{8,10},{10,12},{12,14},{14,16},{16,18},{18... | collective-permute-start | bytes 2359304 | tf_op jit(solution)/shard_map/ppermute | solution.py:14
  20.8 39.8 %collective-permute-start.8 = (bf16[384,512]{0,1:T(8,128)(2,1)S(1)}, bf16[384,512]{0,1:T(8,128)(2,1)S(1)}, u32[]{:S(2)}, u32[]{:S(2)}) collective-permute-start(bf16[384,512]{0,1:T(8,128)(2,1)S(1)} %copy.21), channel_id=1, source_target_pairs={{0,2},{2,4},{4,6},{6,8},{8,10},{10,12},{12,14},{14,16},{16,18},{18... | collective-permute-start | bytes 1179656 | tf_op jit(solution)/shard_map/ppermute | solution.py:14
  24.2 23.4 %collective-permute-start.5 = (s32[384]{0:T(512)S(1)}, s32[384]{0:T(512)S(1)}, u32[]{:S(2)}, u32[]{:S(2)}) collective-permute-start(s32[384]{0:T(512)S(1)} %collective-permute-done.4), channel_id=1, source_target_pairs={{0,2},{2,4},{4,6},{6,8},{8,10},{10,12},{12,14},{14,16},{16,18},{18... | collective-permute-start | bytes 4616 | tf_op jit(solution)/shard_map/ppermute | solution.py:14
  27.6 37.3 %collective-permute-start.13 = (bf16[384,512]{0,1:T(8,128)(2,1)S(1)}, bf16[384,512]{0,1:T(8,128)(2,1)S(1)}, u32[]{:S(2)}, u32[]{:S(2)}) collective-permute-start(bf16[384,512]{0,1:T(8,128)(2,1)S(1)} %collective-permute-done.12), channel_id=1, source_target_pairs={{0,2},{2,4},{4,6},{6,8},{8,10},{10,12},{12,14},{14,16},{16,18},{18... | collective-permute-start | bytes 1179656 | tf_op jit(solution)/shard_map/ppermute | solution.py:14
  47.5 7.3 collective-permute-start.6
  54.9 5.7 collective-permute-start.7
  60.6 13.8 %collective-permute-start.9 = (bf16[384,512]{0,1:T(8,128)(2,1)S(1)}, bf16[384,512]{0,1:T(8,128)(2,1)S(1)}, u32[]{:S(2)}, u32[]{:S(2)}) collective-permute-start(bf16[384,512]{0,1:T(8,128)(2,1)S(1)} %collective-permute-done.8), channel_id=1, source_target_pairs={{0,2},{2,4},{4,6},{6,8},{8,10},{10,12},{12,14},{14,16},{16,18},{18... | collective-permute-start | bytes 1179656 | tf_op jit(solution)/shard_map/ppermute | solution.py:14
  64.9 17.9 %collective-permute-start.14 = (bf16[384,512]{0,1:T(8,128)(2,1)S(1)}, bf16[384,512]{0,1:T(8,128)(2,1)S(1)}, u32[]{:S(2)}, u32[]{:S(2)}) collective-permute-start(bf16[384,512]{0,1:T(8,128)(2,1)S(1)} %collective-permute-done.13), channel_id=1, source_target_pairs={{0,2},{2,4},{4,6},{6,8},{8,10},{10,12},{12,14},{14,16},{16,18},{18... | collective-permute-start | bytes 1179656 | tf_op jit(solution)/shard_map/ppermute | solution.py:14
  74.4 21.5 %collective-permute-start.10 = (bf16[384,512]{0,1:T(8,128)(2,1)S(1)}, bf16[384,512]{0,1:T(8,128)(2,1)}, u32[]{:S(2)}, u32[]{:S(2)}) collective-permute-start(bf16[384,512]{0,1:T(8,128)(2,1)S(1)} %collective-permute-done.9), channel_id=1, source_target_pairs={{0,2},{2,4},{4,6},{6,8},{8,10},{10,12},{12,14},{14,16},{16,18},{18... | collective-permute-start | bytes 1179656 | tf_op jit(solution)/shard_map/ppermute | solution.py:14
  82.8 17.1 %collective-permute-start.15 = (bf16[384,512]{0,1:T(8,128)(2,1)S(1)}, bf16[384,512]{0,1:T(8,128)(2,1)S(1)}, u32[]{:S(2)}, u32[]{:S(2)}) collective-permute-start(bf16[384,512]{0,1:T(8,128)(2,1)S(1)} %collective-permute-done.14), channel_id=1, source_target_pairs={{0,2},{2,4},{4,6},{6,8},{8,10},{10,12},{12,14},{14,16},{16,18},{18... | collective-permute-start | bytes 1179656 | tf_op jit(solution)/shard_map/ppermute | solution.py:14
  90.5 35.3 %collective-permute-start.1 = (bf16[384,1024]{1,0:T(8,128)(2,1)S(1)}, bf16[384,1024]{1,0:T(8,128)(2,1)S(1)}, u32[]{:S(2)}, u32[]{:S(2)}) collective-permute-start(bf16[384,1024]{1,0:T(8,128)(2,1)S(1)} %collective-permute-done), channel_id=1, source_target_pairs={{0,2},{2,4},{4,6},{6,8},{8,10},{10,12},{12,14},{14,16},{16,18},{18... | collective-permute-start | bytes 2359304 | tf_op jit(solution)/shard_map/ppermute | solution.py:14
  95.8 35.5 %collective-permute-start.11 = (bf16[384,512]{0,1:T(8,128)(2,1)}, bf16[384,512]{0,1:T(8,128)(2,1)}, u32[]{:S(2)}, u32[]{:S(2)}) collective-permute-start(bf16[384,512]{0,1:T(8,128)(2,1)} %collective-permute-done.10), channel_id=1, source_target_pairs={{0,2},{2,4},{4,6},{6,8},{8,10},{10,12},{12,14},{14,16},{16,18},{18... | collective-permute-start | bytes 1179656 | tf_op jit(solution)/shard_map/ppermute | solution.py:14
  125.7 17.4 %collective-permute-start.2 = (bf16[384,1024]{1,0:T(8,128)(2,1)S(1)}, bf16[384,1024]{1,0:T(8,128)(2,1)S(1)}, u32[]{:S(2)}, u32[]{:S(2)}) collective-permute-start(bf16[384,1024]{1,0:T(8,128)(2,1)S(1)} %collective-permute-done.1), channel_id=1, source_target_pairs={{0,2},{2,4},{4,6},{6,8},{8,10},{10,12},{12,14},{14,16},{16,18},{18... | collective-permute-start | bytes 2359304 | tf_op jit(solution)/shard_map/ppermute | solution.py:14
  143.1 23.2 %collective-permute-start.3 = (bf16[384,1024]{1,0:T(8,128)(2,1)S(1)}, bf16[384,1024]{1,0:T(8,128)(2,1)S(1)}, u32[]{:S(2)}, u32[]{:S(2)}) collective-permute-start(bf16[384,1024]{1,0:T(8,128)(2,1)S(1)} %collective-permute-done.2), channel_id=1, source_target_pairs={{0,2},{2,4},{4,6},{6,8},{8,10},{10,12},{12,14},{14,16},{16,18},{18... | collective-permute-start | bytes 2359304 | tf_op jit(solution)/shard_map/ppermute | solution.py:14
  193.4 34.1 %all-gather.8.cloned.1.call-start = ((), (), s32[]{:S(2)}) async-start(), calls=%async_computation.2 | async-start | bytes 2359296 | tf_op jit(solution)/shard_map/all_gather | solution.py:88
  216.3 166.5 %all-gather.10.cloned.1.call-start = ((), (), s32[]{:S(2)}) async-start(), calls=%async_computation.3 | async-start | bytes 13369344 | tf_op jit(solution)/shard_map/all_gather | solution.py:91
  217.1 318.1 %all-gather.12.cloned.1.call-start = ((), (), s32[]{:S(2)}) async-start(), calls=%async_computation.4 | async-start | bytes 13369344 | tf_op jit(solution)/shard_map/all_gather | solution.py:96
  217.6 513.7 %all-gather.14.cloned.1.call-start = ((), (), s32[]{:S(2)}) async-start(), calls=%async_computation.5 | async-start | bytes 13369344 | tf_op jit(solution)/shard_map/all_gather | solution.py:102
  218.2 541.4 %reduce-scatter.2.cloned.1.call-start = ((), (), s32[]{:S(2)}) async-start(), calls=%async_computation.6 | async-start | bytes 2359296 | tf_op jit(solution)/shard_map/reduce_scatter | solution.py:105
  227.4 503.9 %copy-start.13 = (bf16[384,2048]{1,0:T(8,128)(2,1)S(1)}, bf16[384,2048]{1,0:T(8,128)(2,1)}, u32[]{:S(2)}) copy-start(bf16[384,2048]{1,0:T(8,128)(2,1)} %all-gather.8.cloned.1.call-done) | copy-start | bytes 4718596
  (14 other events, 293.2 us)
Sparse Core Ops, SparseCore 0:
  193.5 14.5 all-gather.5
  216.4 10.9 all-gather.7
  230.2 152.5 all-gather.9
  385.5 149.5 all-gather.11
  537.7 193.6 all-gather.13
  752.5 7.1 reduce-scatter.1
where the time goes:
time: 770 us; the launch traced here: 769 us
  waiting for transfers between devices  556 us (72%)
  starting transfers between devices  71.9 us (9%)
  matrix products  62.5 us (8%)
  other arithmetic  42.2 us (5%)
  local copies, waits for them, and re-layouts  19.9 us (3%)
  between operations  13.9 us (2%)
    all_gather x1, waiting for transfers between devices, body(): lax.all_gather(down_weight, 'sp', axis=1, tiled=True)  196 us
    all_gather x1, waiting for transfers between devices, body(): lax.all_gather(gate_weight, 'sp', axis=0, tiled=True)  155 us
    all_gather x1, waiting for transfers between devices, body(): lax.all_gather(up_weight, 'sp', axis=0, tiled=True)  142 us
    ppermute x16, starting transfers between devices, shifted(): return lax.ppermute(value, axis, pairs)  71.5 us
    sub x2, other arithmetic, weights(): score = score - jnp.max(score, axis=-1, keepdims=True)  35.1 us
    ppermute x16, waiting for transfers between devices, shifted(): return lax.ppermute(value, axis, pairs)  29.3 us
    dot_general x1, matrix products, body(): jnp.dot(hidden, lax.all_gather(down_weight, 'sp', axis=1, tiled=True), pr...  21 us
  transfers between devices with their start and end apart: 22, of which 12 were waited for; matrix products, arithmetic and copies ran while one was open for 9% of the time, Pallas kernels for 0%

commit v1 on v0

--- a/solution.py
+++ b/solution.py
@@ -99,7 +99,7 @@
     hidden = (jax.nn.silu(gate) * up).astype(jnp.bfloat16)
     terms = jnp.dot(
         hidden,
-        lax.all_gather(down_weight, "sp", axis=1, tiled=True),
+        jnp.concatenate(lax.all_gather(down_weight, "sp"), axis=1),
         preferred_element_type=jnp.float32,
     )
     summed = lax.psum_scatter(

time: 770 us -> 715 us (0.929)
  waiting for transfers between devices: 556 us -> 489 us
  local copies, waits for them, and re-layouts: 19.9 us -> 36.6 us
    all_gather x1, waiting for transfers between devices: 196 us -> 146 us  [body(): lax.all_gather(down_weight, 'sp')]
    reshape x0 -> x1, local copies, waits for them, and re-layouts: none -> 16.7 us  [body(): jnp.concatenate(lax.all_gather(down_weight, 'sp'), axis=1)]
    all_gather x1, waiting for transfers between devices: 9.18 us -> 0.01 us  [body(): whole_rows = lax.all_gather(normed, 'tp', axis=1, tiled=True)]
  transfers between devices with their start and end apart: 22 -> 22, of which waited for: 12 -> 11; matrix products, arithmetic and copies ran while one was open for 9% -> 13% of each run, Pallas kernels for 0% -> 0%
where the time goes in v1:
time: 715 us; the launch traced here: 713 us
  waiting for transfers between devices  489 us (68%)
  starting transfers between devices  71.9 us (10%)
  matrix products  57.7 us (8%)
  other arithmetic  42.2 us (6%)
  local copies, waits for them, and re-layouts  36.6 us (5%)
  between operations  13.9 us (2%)
    all_gather x1, waiting for transfers between devices, body(): lax.all_gather(gate_weight, 'sp', axis=0, tiled=True)  148 us
    all_gather x1, waiting for transfers between devices, body(): lax.all_gather(down_weight, 'sp')  146 us
    all_gather x1, waiting for transfers between devices, body(): lax.all_gather(up_weight, 'sp', axis=0, tiled=True)  142 us
    ppermute x16, starting transfers between devices, shifted(): return lax.ppermute(value, axis, pairs)  71.5 us
    sub x2, other arithmetic, weights(): score = score - jnp.max(score, axis=-1, keepdims=True)  35 us
    ppermute x16, waiting for transfers between devices, shifted(): return lax.ppermute(value, axis, pairs)  29.3 us
    reshape x1, local copies, waits for them, and re-layouts, body(): jnp.concatenate(lax.all_gather(down_weight, 'sp'), axis=1)  16.7 us
    dot_general x1, matrix products, body(): jnp.dot(hidden, jnp.concatenate(lax.all_gather(down_weight, 'sp'), axis=1...  16.3 us
  transfers between devices with their start and end apart: 22, of which 11 were waited for; matrix products, arithmetic and copies ran while one was open for 13% of the time, Pallas kernels for 0%

profile of v1, /device:TPU:0, one launch (start us, length us, event | category | flops | bytes accessed | tf_op | source)
XLA Modules:
  0.0 713.3 jit_solution(3571459627119220905)
XLA Ops:
  7.8 4.9 collective-permute-start.12
  31.0 16.5 %collective-permute-done.5 = s32[384]{0:T(512)S(1)} collective-permute-done((s32[384]{0:T(512)S(1)}, s32[384]{0:T(512)S(1)}, u32[]{:S(2)}, u32[]{:S(2)}) %collective-permute-start.5) | collective-permute-done | bytes 1568 | tf_op jit(solution)/shard_map/ppermute | solution.py:14
  64.9 5.1 collective-permute-start.14
  74.4 5.9 collective-permute-start.10
  82.8 5.1 collective-permute-start.15
  90.5 5.3 collective-permute-start.1
  102.2 6.2 fusion.19
  108.4 17.4 %fusion.30 = (f32[4,384]{1,0:T(4,128)S(1)}, f32[4,384,1920]{1,2,0:T(8,128)}) fusion(f32[4,1920,384]{2,1,0:T(8,128)} %fusion.19, pred[384,1920]{0,1:T(8,128)(4,1)S(1)} %and_and_fusion), kind=kOutput, calls=%fused_computation.71 | output fusion | flops 17696640 | bytes 24336384 | tf_op jit(solution)/shard_map/sub | solution.py:59
  125.7 5.6 collective-permute-start.2
  134.7 6.1 fusion.22
  143.1 5.5 collective-permute-start.3
  148.6 17.7 %fusion.31 = (f32[4,384]{1,0:T(4,128)S(1)}, f32[4,384,1920]{1,2,0:T(8,128)}) fusion(f32[4,1920,384]{2,1,0:T(8,128)} %fusion.22, pred[384,1920]{0,1:T(8,128)(4,1)} %copy-done.4), kind=kOutput, calls=%fused_computation.72 | output fusion | flops 17696640 | bytes 24336384 | tf_op jit(solution)/shard_map/sub | solution.py:59
  171.1 6.3 copy.31
  177.4 8.0 %fusion.9 = f32[4,256,384]{2,1,0:T(8,128)S(1)} fusion(bf16[1920,4,256]{0,2,1:T(8,128)(2,1)} %bitcast.66, f32[4,384,1920]{1,2,0:T(8,128)} %get-tuple-element.6, f32[4,384]{1,0:T(4,128)S(1)} %get-tuple-element.5), kind=kOutput, calls=%fused_computation.15 | convolution fusion | flops 1515847680 | bytes 17307648 | tf_op jit(solution)/shard_map/hqk,khe->qhe/dot_general | solution.py:66
  185.4 6.7 fusion.16
  194.3 13.7 %all-gather.7.cloned.1.call-done = bf16[384,2048]{0,1:T(8,128)(2,1)} async-done(((bf16[384,1024]{0,1:T(8,128)(2,1)}), bf16[384,2048]{0,1:T(8,128)(2,1)}) %all-gather.7.cloned.1.call-update) | async-done | bytes 1572880 | tf_op jit(solution)/shard_map/all_gather | solution.py:77
  208.0 4.6 fusion.12
  217.4 145.9 %all-gather.15.cloned.1.call-done = bf16[49152,128]{1,0:T(8,128)(2,1)} async-done(((bf16[3072,128]{1,0:T(8,128)(2,1)}), bf16[49152,128]{1,0:T(8,128)(2,1)}) %all-gather.15.cloned.1.call-update) | async-done | bytes 12582928 | tf_op jit(solution)/shard_map/all_gather | solution.py:102
  363.4 16.7 %copy.42 = bf16[3072,16,128]{0,2,1:T(8,128)(2,1)} copy(bf16[3072,16,128]{2,0,1:T(8,128)(2,1)} %bitcast.64) | data formatting | bytes 25165824 | tf_op jit(solution)/shard_map/reshape | solution.py:102
  380.1 148.1 %all-gather.11.cloned.1.call-done = bf16[2048,3072]{1,0:T(8,128)(2,1)} async-done(((bf16[128,3072]{1,0:T(8,128)(2,1)}), bf16[2048,3072]{1,0:T(8,128)(2,1)}) %all-gather.11.cloned.1.call-update) | async-done | bytes 12582928 | tf_op jit(solution)/shard_map/all_gather | solution.py:91
  528.2 9.9 %fusion.32 = f32[384,3072]{1,0:T(8,128)} fusion(bf16[384,2048]{1,0:T(8,128)(2,1)} %all-gather.9.cloned.1.call-done, bf16[2048,3072]{1,0:T(8,128)(2,1)} %all-gather.11.cloned.1.call-done), kind=kOutput, calls=%fused_computation.73 | convolution fusion | flops 4831838208 | bytes 18874368 | tf_op jit(solution)/shard_map/dot_general | solution.py:89
  538.0 142.4 %all-gather.13.cloned.1.call-done = bf16[2048,3072]{1,0:T(8,128)(2,1)} async-done(((bf16[128,3072]{1,0:T(8,128)(2,1)}), bf16[2048,3072]{1,0:T(8,128)(2,1)}) %all-gather.13.cloned.1.call-update) | async-done | bytes 12582928 | tf_op jit(solution)/shard_map/all_gather | solution.py:96
  680.4 16.3 %convolution_convert_fusion = bf16[384,2048]{1,0:T(8,128)(2,1)} fusion(bf16[3072,2048]{0,1:T(8,128)(2,1)} %bitcast.65, f32[384,3072]{1,0:T(8,128)} %fusion.32, bf16[384,2048]{1,0:T(8,128)(2,1)S(1)} %copy-done.13, bf16[2048,3072]{1,0:T(8,128)(2,1)} %all-gather.13.cloned.1.call-done), kind=kOutput, calls=%fused_computation.20 | convolution fusion | flops 9671540736 | bytes 33030144 | tf_op jit(solution)/shard_map/dot_general | solution.py:100
  696.8 7.3 %reduce-scatter.2.cloned.1.call-done = bf16[384,1024]{1,0:T(8,128)(2,1)} async-done(((bf16[384,2048]{1,0:T(8,128)(2,1)}), bf16[384,1024]{1,0:T(8,128)(2,1)}) %reduce-scatter.2.cloned.1.call-update) | async-done | bytes 786448 | tf_op jit(solution)/shard_map/reduce_scatter | solution.py:105
  (102 shorter events, 72.3 us)
Async XLA Ops:
  6.5 95.7 %copy-start = (bf16[384,512]{1,0:T(8,128)(2,1)S(1)}, bf16[384,512]{1,0:T(8,128)(2,1)}, u32[]{:S(2)}) copy-start(bf16[384,512]{1,0:T(8,128)(2,1)} %param.17) | copy-start | bytes 1179652
  6.5 201.4 %all-gather.7.cloned.1.call-start = ((), (), s32[]{:S(2)}) async-start(), calls=%async_computation.1 | async-start | bytes 2359296 | tf_op jit(solution)/shard_map/all_gather | solution.py:77
  7.8 19.7 %collective-permute-start.12 = (bf16[384,512]{0,1:T(8,128)(2,1)S(1)}, bf16[384,512]{0,1:T(8,128)(2,1)S(1)}, u32[]{:S(2)}, u32[]{:S(2)}) collective-permute-start(bf16[384,512]{0,1:T(8,128)(2,1)S(1)} %copy.37), channel_id=1, source_target_pairs={{0,2},{2,4},{4,6},{6,8},{8,10},{10,12},{12,14},{14,16},{16,18},{18... | collective-permute-start | bytes 1179656 | tf_op jit(solution)/shard_map/ppermute | solution.py:14
  12.7 11.4 %collective-permute-start.4 = (s32[384]{0:T(512)}, s32[384]{0:T(512)S(1)}, u32[]{:S(2)}, u32[]{:S(2)}) collective-permute-start(s32[384]{0:T(512)} %param.21), channel_id=1, source_target_pairs={{0,2},{2,4},{4,6},{6,8},{8,10},{10,12},{12,14},{14,16},{16,18},{18... | collective-permute-start | bytes 4616 | tf_op jit(solution)/shard_map/ppermute | solution.py:14
  16.1 74.4 %collective-permute-start = (bf16[384,1024]{1,0:T(8,128)(2,1)}, bf16[384,1024]{1,0:T(8,128)(2,1)S(1)}, u32[]{:S(2)}, u32[]{:S(2)}) collective-permute-start(bf16[384,1024]{1,0:T(8,128)(2,1)} %param.19), channel_id=1, source_target_pairs={{0,2},{2,4},{4,6},{6,8},{8,10},{10,12},{12,14},{14,16},{16,18},{18... | collective-permute-start | bytes 2359304 | tf_op jit(solution)/shard_map/ppermute | solution.py:14
  20.8 39.8 %collective-permute-start.8 = (bf16[384,512]{0,1:T(8,128)(2,1)S(1)}, bf16[384,512]{0,1:T(8,128)(2,1)S(1)}, u32[]{:S(2)}, u32[]{:S(2)}) collective-permute-start(bf16[384,512]{0,1:T(8,128)(2,1)S(1)} %copy.32), channel_id=1, source_target_pairs={{0,2},{2,4},{4,6},{6,8},{8,10},{10,12},{12,14},{14,16},{16,18},{18... | collective-permute-start | bytes 1179656 | tf_op jit(solution)/shard_map/ppermute | solution.py:14
  24.2 23.4 %collective-permute-start.5 = (s32[384]{0:T(512)S(1)}, s32[384]{0:T(512)S(1)}, u32[]{:S(2)}, u32[]{:S(2)}) collective-permute-start(s32[384]{0:T(512)S(1)} %collective-permute-done.4), channel_id=1, source_target_pairs={{0,2},{2,4},{4,6},{6,8},{8,10},{10,12},{12,14},{14,16},{16,18},{18... | collective-permute-start | bytes 4616 | tf_op jit(solution)/shard_map/ppermute | solution.py:14
  27.6 37.3 %collective-permute-start.13 = (bf16[384,512]{0,1:T(8,128)(2,1)S(1)}, bf16[384,512]{0,1:T(8,128)(2,1)S(1)}, u32[]{:S(2)}, u32[]{:S(2)}) collective-permute-start(bf16[384,512]{0,1:T(8,128)(2,1)S(1)} %collective-permute-done.12), channel_id=1, source_target_pairs={{0,2},{2,4},{4,6},{6,8},{8,10},{10,12},{12,14},{14,16},{16,18},{18... | collective-permute-start | bytes 1179656 | tf_op jit(solution)/shard_map/ppermute | solution.py:14
  47.5 7.3 %collective-permute-start.6 = (s32[384]{0:T(512)S(1)}, s32[384]{0:T(512)S(1)}, u32[]{:S(2)}, u32[]{:S(2)}) collective-permute-start(s32[384]{0:T(512)S(1)} %collective-permute-done.5), channel_id=1, source_target_pairs={{0,2},{2,4},{4,6},{6,8},{8,10},{10,12},{12,14},{14,16},{16,18},{18... | collective-permute-start | bytes 4616 | tf_op jit(solution)/shard_map/ppermute | solution.py:14
  54.9 5.7 collective-permute-start.7
  60.6 13.8 %collective-permute-start.9 = (bf16[384,512]{0,1:T(8,128)(2,1)S(1)}, bf16[384,512]{0,1:T(8,128)(2,1)S(1)}, u32[]{:S(2)}, u32[]{:S(2)}) collective-permute-start(bf16[384,512]{0,1:T(8,128)(2,1)S(1)} %collective-permute-done.8), channel_id=1, source_target_pairs={{0,2},{2,4},{4,6},{6,8},{8,10},{10,12},{12,14},{14,16},{16,18},{18... | collective-permute-start | bytes 1179656 | tf_op jit(solution)/shard_map/ppermute | solution.py:14
  64.9 17.9 %collective-permute-start.14 = (bf16[384,512]{0,1:T(8,128)(2,1)S(1)}, bf16[384,512]{0,1:T(8,128)(2,1)S(1)}, u32[]{:S(2)}, u32[]{:S(2)}) collective-permute-start(bf16[384,512]{0,1:T(8,128)(2,1)S(1)} %collective-permute-done.13), channel_id=1, source_target_pairs={{0,2},{2,4},{4,6},{6,8},{8,10},{10,12},{12,14},{14,16},{16,18},{18... | collective-permute-start | bytes 1179656 | tf_op jit(solution)/shard_map/ppermute | solution.py:14
  74.4 21.5 %collective-permute-start.10 = (bf16[384,512]{0,1:T(8,128)(2,1)S(1)}, bf16[384,512]{0,1:T(8,128)(2,1)}, u32[]{:S(2)}, u32[]{:S(2)}) collective-permute-start(bf16[384,512]{0,1:T(8,128)(2,1)S(1)} %collective-permute-done.9), channel_id=1, source_target_pairs={{0,2},{2,4},{4,6},{6,8},{8,10},{10,12},{12,14},{14,16},{16,18},{18... | collective-permute-start | bytes 1179656 | tf_op jit(solution)/shard_map/ppermute | solution.py:14
  82.8 17.1 %collective-permute-start.15 = (bf16[384,512]{0,1:T(8,128)(2,1)S(1)}, bf16[384,512]{0,1:T(8,128)(2,1)S(1)}, u32[]{:S(2)}, u32[]{:S(2)}) collective-permute-start(bf16[384,512]{0,1:T(8,128)(2,1)S(1)} %collective-permute-done.14), channel_id=1, source_target_pairs={{0,2},{2,4},{4,6},{6,8},{8,10},{10,12},{12,14},{14,16},{16,18},{18... | collective-permute-start | bytes 1179656 | tf_op jit(solution)/shard_map/ppermute | solution.py:14
  90.5 35.3 %collective-permute-start.1 = (bf16[384,1024]{1,0:T(8,128)(2,1)S(1)}, bf16[384,1024]{1,0:T(8,128)(2,1)S(1)}, u32[]{:S(2)}, u32[]{:S(2)}) collective-permute-start(bf16[384,1024]{1,0:T(8,128)(2,1)S(1)} %collective-permute-done), channel_id=1, source_target_pairs={{0,2},{2,4},{4,6},{6,8},{8,10},{10,12},{12,14},{14,16},{16,18},{18... | collective-permute-start | bytes 2359304 | tf_op jit(solution)/shard_map/ppermute | solution.py:14
  95.8 35.5 %collective-permute-start.11 = (bf16[384,512]{0,1:T(8,128)(2,1)}, bf16[384,512]{0,1:T(8,128)(2,1)}, u32[]{:S(2)}, u32[]{:S(2)}) collective-permute-start(bf16[384,512]{0,1:T(8,128)(2,1)} %collective-permute-done.10), channel_id=1, source_target_pairs={{0,2},{2,4},{4,6},{6,8},{8,10},{10,12},{12,14},{14,16},{16,18},{18... | collective-permute-start | bytes 1179656 | tf_op jit(solution)/shard_map/ppermute | solution.py:14
  125.7 17.4 %collective-permute-start.2 = (bf16[384,1024]{1,0:T(8,128)(2,1)S(1)}, bf16[384,1024]{1,0:T(8,128)(2,1)S(1)}, u32[]{:S(2)}, u32[]{:S(2)}) collective-permute-start(bf16[384,1024]{1,0:T(8,128)(2,1)S(1)} %collective-permute-done.1), channel_id=1, source_target_pairs={{0,2},{2,4},{4,6},{6,8},{8,10},{10,12},{12,14},{14,16},{16,18},{18... | collective-permute-start | bytes 2359304 | tf_op jit(solution)/shard_map/ppermute | solution.py:14
  143.1 23.2 %collective-permute-start.3 = (bf16[384,1024]{1,0:T(8,128)(2,1)S(1)}, bf16[384,1024]{1,0:T(8,128)(2,1)S(1)}, u32[]{:S(2)}, u32[]{:S(2)}) collective-permute-start(bf16[384,1024]{1,0:T(8,128)(2,1)S(1)} %collective-permute-done.2), channel_id=1, source_target_pairs={{0,2},{2,4},{4,6},{6,8},{8,10},{10,12},{12,14},{14,16},{16,18},{18... | collective-permute-start | bytes 2359304 | tf_op jit(solution)/shard_map/ppermute | solution.py:14
  193.2 170.1 %all-gather.15.cloned.1.call-start = ((), (), s32[]{:S(2)}) async-start(), calls=%async_computation.6 | async-start | bytes 13369344 | tf_op jit(solution)/shard_map/all_gather | solution.py:102
  194.0 186.1 %all-gather.9.cloned.1.call-start = ((), (), s32[]{:S(2)}) async-start(), calls=%async_computation.2 | async-start | bytes 2359296 | tf_op jit(solution)/shard_map/all_gather | solution.py:88
  216.2 312.0 %all-gather.11.cloned.1.call-start = ((), (), s32[]{:S(2)}) async-start(), calls=%async_computation.3 | async-start | bytes 13369344 | tf_op jit(solution)/shard_map/all_gather | solution.py:91
  216.8 463.6 %all-gather.13.cloned.1.call-start = ((), (), s32[]{:S(2)}) async-start(), calls=%async_computation.4 | async-start | bytes 13369344 | tf_op jit(solution)/shard_map/all_gather | solution.py:96
  217.4 486.7 %reduce-scatter.2.cloned.1.call-start = ((), (), s32[]{:S(2)}) async-start(), calls=%async_computation.5 | async-start | bytes 2359296 | tf_op jit(solution)/shard_map/reduce_scatter | solution.py:105
  380.1 300.4 %copy-start.13 = (bf16[384,2048]{1,0:T(8,128)(2,1)S(1)}, bf16[384,2048]{1,0:T(8,128)(2,1)}, u32[]{:S(2)}) copy-start(bf16[384,2048]{1,0:T(8,128)(2,1)} %all-gather.9.cloned.1.call-done) | copy-start | bytes 4718596
  (14 other events, 280.9 us)
Sparse Core Ops, SparseCore 0:
  193.4 14.5 all-gather.6
  210.7 152.5 all-gather.14
  364.9 7.9 all-gather.8
  375.6 152.5 all-gather.10
  530.8 149.5 all-gather.12
  696.9 7.1 reduce-scatter.1
